TPU v7x, 32 devices: a whole 2x2x4 slice. The times are simulated.
32 devices in a mesh: grp: 2 (over y), kv: 4 (over z), tp: 4 (over x, core).
Axes of the slice: x: 2, y: 2, z: 4, core: 2. Of those that a mesh axis runs over, the one named last changes fastest.
Arguments:
- tokens: bfloat16 [4096, 2048], P(('grp', 'kv')), parts along dimension 0, may hold values from -72 to 72
- w_query: bfloat16 [2048, 1024], P(None, 'tp'), may hold values from -0.125 to 0.125
- w_key: bfloat16 [2048, 256], P(None, 'tp'), may hold values from -0.125 to 0.125
- w_value: bfloat16 [2048, 256], P(None, 'tp'), may hold values from -0.125 to 0.125
- w_out: bfloat16 [1024, 2048], P('tp'), may hold values from -0.1875 to 0.1875
- selection: int32 [4, 64, 32], P('tp', ('grp', 'kv')), parts along dimension 1, may hold values from -1 to 31, as said below
Outputs:
- attended_out: bfloat16 [4096, 2048], P(('grp', 'kv', 'tp')), parts along dimension 0
There are 2 independent parts, one for each index of `grp`. A program takes and returns all parts, laid end to end along the dimension named above; an argument that names none is the same for every part. Nothing has to cross between parts.
Inputs may be any that keep to these rules, and one draw needn't show every extreme that they name: `selection`: entry 0 is the query block's own index; the others are distinct indices of earlier blocks, then -1 for unused entries. For one key head, the query blocks of one device's range together choose at most 2 distinct blocks of any other device's range, and some device reaches 2 in every draw.
All inputs are finite; a program needn't handle non-finite values.
Results may differ from a plain program's by a relative error of at most 0.028.
The roundings to bfloat16 on the way count: a program that leaves them out, or rounds other values in their place, can miss the bound.
Values may be sent and summed in bfloat16 or wider, within the bound.
A program may use at most 128 MiB of HBM per device.

v0:
```python
import functools

import jax
import jax.numpy as jnp
import numpy as np
from jax import lax
from jax.experimental import pallas as pl
from jax.experimental.pallas import tpu as pltpu
from jax.sharding import PartitionSpec as P

HEAD_DIM = 64
BLOCK = 64
ROPE_BASE = 500000.0
NEG = -1e30
CHUNKS = 4
TOK_PARTS = 4
MESH = pl.DeviceIdType.MESH
NT = (((1,), (1,)), ((), ()))


def tables(n_blocks):
    half = HEAD_DIM // 2
    lane = np.arange(128)
    freqs = ROPE_BASE ** (-(lane % half).astype(np.float64) / half)
    sign = np.where(lane % HEAD_DIM < half, -1.0, 1.0)
    inner = np.arange(BLOCK)[:, None] * freqs
    outer = (np.arange(n_blocks) * BLOCK)[:, None] * freqs
    inside = np.stack([np.cos(inner), np.sin(inner), sign * np.cos(inner), sign * np.sin(inner)])
    outside = np.stack([np.cos(outer), np.sin(outer)])
    return inside.astype(np.float32), outside.astype(np.float32)


def kernel(
    n, n_tp, n_grp,
    tok_h, wq_h, wk_h, wv_h, wo_h, sel_h, in_h, out_tab_h,
    o_ref,
    in_ref, out_tab_ref, tok, wq, w_kv, wfull, sel_all, qf, kv_own, send_kv, recv_kv,
    bias_l, bias_r, acc_s, max_s, qs_s, att, att_in, total_s,
    in_sem, sel_ss, sel_rs, kv_ss, kv_rs, w_ss, w_rs, d_ss, d_rs, near_ss, near_rs, a_ss, a_rs,
):
    grp = lax.axis_index("grp")
    me = lax.axis_index("kv")
    t = lax.axis_index("tp")
    rows = tok.shape[0]
    blocks = rows // BLOCK
    heads = wq.shape[1] // HEAD_DIM
    topk = sel_all.shape[2]
    group_rows = heads * BLOCK
    far = lax.rem(t + n_tp // 2, n_tp)
    near = t + 1 - 2 * lax.rem(t, 2)
    other = n_grp - 1 - grp
    width = wo_h.shape[0]
    side = lax.rem(me, 2)
    beside = me + 1 - 2 * side
    mine, from_y, from_z, last_part = grp * 2 + side, other * 2 + side, grp * 2 + 1 - side, other * 2 + 1 - side
    parts = (mine, from_y, from_z, last_part)
    quarter = width // (2 * n_grp)
    piece = quarter // CHUNKS
    tok_rows = rows // TOK_PARTS

    def local(src, dst, k):
        return pltpu.make_async_copy(src, dst, in_sem.at[k])

    loads = [
        local(wk_h, w_kv.at[:HEAD_DIM], 0), local(wv_h, w_kv.at[HEAD_DIM:], 1), local(in_h, in_ref, 2),
        local(sel_h.at[0], sel_all.at[me], 3), local(wq_h, wq, 4), local(wo_h, wfull.at[t], 5),
        local(out_tab_h, out_tab_ref, 6),
    ]
    tok_loads = []
    for k in range(TOK_PARTS):
        part = pl.ds(k * tok_rows, tok_rows)
        tok_loads.append(local(tok_h.at[part], tok.at[part], 7 + k))
    for load in loads[:2] + tok_loads + [loads[2], loads[6], loads[3], loads[4]]:
        load.start()

    barrier = pltpu.get_barrier_semaphore()
    for k in range(1, n_tp):
        pl.semaphore_signal(barrier, inc=1, device_id={"tp": lax.rem(t + k, n_tp)}, device_id_type=MESH)
    for k in range(1, n_grp):
        pl.semaphore_signal(barrier, inc=1, device_id={"grp": lax.rem(grp + k, n_grp)}, device_id_type=MESH)
    for k in range(1, n):
        pl.semaphore_signal(barrier, inc=1, device_id={"kv": lax.rem(me + k, n)}, device_id_type=MESH)
    pl.semaphore_wait(barrier, n_tp + n_grp + n - 3)

    def remote(src, dst, ss, rs, axis, index):
        return pltpu.make_async_remote_copy(
            src_ref=src, dst_ref=dst, send_sem=ss, recv_sem=rs,
            device_id={axis: index}, device_id_type=MESH,
        )

    def piece_of(part_of, c):
        return pl.ds(part_of * quarter + c * piece, piece)

    def x_copy(kind, c, owner):
        at = piece_of(parts[kind], c)
        return remote(wo_h.at[at], wfull.at[owner, at], w_ss.at[kind, c], w_rs.at[kind, c], "tp", far)

    def link_copy(kind, c, part_of):
        piece_at = wfull.at[far, piece_of(part_of, c)]
        along_y = kind == 1 or (kind == 3 and c % 2 == 0)
        axis, to = ("grp", other) if along_y else ("kv", beside)
        return remote(piece_at, piece_at, w_ss.at[kind, c], w_rs.at[kind, c], axis, to)

    def near_copy(kind, c, owner):
        piece_at = wfull.at[owner, piece_of(parts[kind], c)]
        return remote(piece_at, piece_at, near_ss.at[kind, c], near_rs.at[kind, c], "tp", near)

    def own_copy(owner):
        return remote(wo_h, wfull.at[owner], d_ss, d_rs, "tp", near)

    def sel_copy(source, to):
        return remote(sel_h.at[0], sel_all.at[source], sel_ss.at[to], sel_rs.at[source], "kv", to)

    def kv_copy(source, to):
        return remote(send_kv.at[to], recv_kv.at[source], kv_ss.at[to], kv_rs.at[source], "kv", to)

    for s in range(n - 1):
        @pl.when(s < me)
        def _():
            sel_copy(me, s).start()
    for c in range(CHUNKS):
        x_copy(0, c, t).start()
    for c in range(CHUNKS // 2, CHUNKS):
        x_copy(3, c, t).start()

    for s in range(n - 1):
        @pl.when(s >= me)
        def _():
            recv_kv[s] = jnp.zeros(recv_kv.shape[1:], recv_kv.dtype)

    lane = lax.broadcasted_iota(jnp.int32, (BLOCK, 128), 1)
    low = lane < HEAD_DIM
    first = lax.rem(lane, HEAD_DIM) < HEAD_DIM // 2

    def angle(i):
        at = me * blocks + i
        cos_b = out_tab_ref[0, pl.ds(at, 1), :]
        sin_b = out_tab_ref[1, pl.ds(at, 1), :]
        return in_ref[0] * cos_b - in_ref[1] * sin_b, in_ref[3] * cos_b + in_ref[2] * sin_b

    def rotated(x, cos, sin):
        swapped = jnp.where(first, pltpu.roll(x, 96, 1), pltpu.roll(x, 32, 1))
        return x * cos + swapped * sin

    loads[0].wait()
    loads[1].wait()
    loads[2].wait()
    loads[6].wait()
    per_part = tok_rows // BLOCK
    for i in range(blocks):
        if i % per_part == 0:
            tok_loads[i // per_part].wait()
            at = i * BLOCK
            qf[at:at + tok_rows, :128] = lax.dot_general(
                tok[at:at + tok_rows, :], w_kv[...], NT, preferred_element_type=jnp.float32
            )
        cos, sin = angle(i)
        x = qf[i * BLOCK:(i + 1) * BLOCK, :128]
        turned = rotated(x, jnp.where(low, cos, 1.0), jnp.where(low, sin, 0.0))
        kv_own[i * BLOCK:(i + 1) * BLOCK, :] = turned.astype(jnp.bfloat16)

    def ends(sel, source):
        e = sel - source * blocks
        inside = (e >= 0) & (e < blocks)
        ef = e.astype(jnp.float32)
        lo = jnp.where(inside, ef, 1e6)
        hi = jnp.where(inside, ef, -1e6)
        lo = jnp.min(jnp.min(lo, axis=1, keepdims=True), axis=0, keepdims=True)
        hi = jnp.max(jnp.max(hi, axis=1, keepdims=True), axis=0, keepdims=True)
        return lo, hi

    loads[3].wait()
    r_iota = lax.broadcasted_iota(jnp.int32, (2 * BLOCK, rows), 0)
    c_iota = lax.broadcasted_iota(jnp.int32, (2 * BLOCK, rows), 1)
    r_in = lax.rem(r_iota, BLOCK).astype(jnp.float32)
    c_f = c_iota.astype(jnp.float32)
    for r in range(n - 1, 0, -1):
        @pl.when(r > me)
        def _():
            sel_copy(r, r).wait_recv()
            lo, hi = ends(sel_all[r], me)
            want = jnp.where(r_iota < BLOCK, lo, hi) * BLOCK + r_in
            pick = jnp.where(c_f == want, 1.0, 0.0).astype(jnp.bfloat16)
            chosen = jnp.dot(pick, kv_own[...], preferred_element_type=jnp.float32)
            send_kv[r] = chosen.astype(jnp.bfloat16)
            kv_copy(me, r).start()

    loads[5].start()
    own_copy(t).start()

    loads[4].wait()
    qf[...] = jnp.dot(tok[...], wq[...], preferred_element_type=jnp.float32)

    sel_f = sel_all[me].astype(jnp.float32)
    base = (me * blocks).astype(jnp.float32)
    local_id = (lax.broadcasted_iota(jnp.int32, (blocks, rows), 1) // BLOCK).astype(jnp.float32) + base
    hit = jnp.zeros((blocks, rows), jnp.float32)
    for k in range(topk):
        hit = jnp.where(sel_f[:, k:k + 1] == local_id, 1.0, hit)
    bias_l[...] = jnp.where(hit > 0.5, 0.0, NEG)

    slot = lax.broadcasted_iota(jnp.int32, (blocks, 2 * BLOCK), 1)
    for s in range(n - 1):
        lo, hi = ends(sel_all[me], s)
        ident = jnp.where(slot < BLOCK, lo, jnp.where(hi != lo, hi, -1e6)) + (s * blocks)
        hit = jnp.zeros((blocks, 2 * BLOCK), jnp.float32)
        for k in range(topk):
            hit = jnp.where(sel_f[:, k:k + 1] == ident, 1.0, hit)
        bias_r[s] = jnp.where((hit > 0.5) & (s < me), 0.0, NEG)

    def with_ones(kv):
        at = lax.broadcasted_iota(jnp.int32, kv.shape, 1)
        return jnp.where(at < HEAD_DIM, jnp.ones_like(kv), kv)

    q_row = lax.rem(lax.broadcasted_iota(jnp.int32, (group_rows, 128), 0), BLOCK)
    q_col = lax.broadcasted_iota(jnp.int32, (group_rows, 128), 1)
    zero = jnp.zeros((BLOCK, 128), jnp.float32)

    def pass_on(c):
        x_copy(0, c, far).wait_recv()
        link_copy(1, c, mine).start()
        link_copy(2, c, mine).start()
        near_copy(0, c, far).start()

    def pass_late(c):
        link_copy(1, c, from_y).wait_recv()
        link_copy(2, c, from_z).wait_recv()
        if c < CHUNKS // 2:
            link_copy(3, c, from_z if c % 2 == 0 else from_y).start()
        near_copy(1, c, far).start()
        near_copy(2, c, far).start()

    def pass_last(c):
        if c < CHUNKS // 2:
            link_copy(3, c, last_part).wait_recv()
        else:
            x_copy(3, c, far).wait_recv()
        near_copy(3, c, far).start()

    pass_on(0)
    for i in range(blocks):
        cos, sin = angle(i)
        cos, sin = cos * HEAD_DIM ** -0.5, sin * HEAD_DIM ** -0.5
        stacked = []
        for pair in range(heads // 2):
            turned = rotated(qf[i * BLOCK:(i + 1) * BLOCK, pair * 128:(pair + 1) * 128], cos, sin)
            stacked.append(jnp.where(low, turned, zero))
            stacked.append(jnp.where(low, pltpu.roll(turned, HEAD_DIM, 1), zero))
        qs = jnp.concatenate(stacked, axis=0).astype(jnp.bfloat16)
        qs_s[i] = qs
        keys = 128 * (i // 2 + 1)
        kv = kv_own[:keys, :]
        scores = lax.dot_general(qs, kv, NT, preferred_element_type=jnp.float32)
        scores = scores + bias_l[i:i + 1, :keys]
        last = jnp.where(q_col <= q_row + (i % 2) * BLOCK, scores[:, keys - 128:], NEG)
        scores = last if keys == 128 else jnp.concatenate([scores[:, :keys - 128], last], axis=1)
        top = jnp.max(scores, axis=1, keepdims=True)
        p = jnp.exp(scores - top).astype(jnp.bfloat16)
        acc_s[i] = jnp.dot(p, with_ones(kv), preferred_element_type=jnp.float32)
        max_s[i] = jnp.broadcast_to(top, (group_rows, 128))
        if i % 2 == 1 and i // 2 + 1 < CHUNKS:
            pass_on(i // 2 + 1)
    pass_late(0)

    for s in range(n - 1):
        @pl.when(s < me)
        def _():
            kv_copy(s, s).wait_recv()

    step = max(k for k in (1, 2, 3, 4) if (n - 1) % k == 0)

    def remote_part(at, i):
        kv = recv_kv[pl.ds(at * step, step)].reshape(step * 128, 128)
        scores = lax.dot_general(qs_s[i], kv, NT, preferred_element_type=jnp.float32)
        scores = jnp.concatenate(
            [scores[:, k * 128:(k + 1) * 128] + bias_r[at * step + k, pl.ds(i, 1), :] for k in range(step)], axis=1
        )
        before = max_s[i]
        top = jnp.maximum(before[:, :1], jnp.max(scores, axis=1, keepdims=True))
        p = jnp.exp(scores - top).astype(jnp.bfloat16)
        acc_s[i] = acc_s[i] * jnp.exp(before - top) + jnp.dot(
            p, with_ones(kv), preferred_element_type=jnp.float32
        )
        if n - 1 > step:
            max_s[i] = jnp.broadcast_to(top, (group_rows, 128))

    per = blocks // n_tp

    def att_copy(owner, to):
        return remote(att.at[to], att_in.at[owner], a_ss.at[to], a_rs.at[owner], "tp", to)

    far_near = lax.rem(near + n_tp // 2, n_tp)
    for turn, d in enumerate((far, far_near, near, t)):
        for b in range(per):
            i = d * per + b

            @pl.when(me > 0)
            def _():
                if n - 1 > step:
                    lax.fori_loop(0, (n - 1) // step, lambda at, _: (remote_part(at, i), 0)[1], 0)
                else:
                    remote_part(0, i)

            for pair in range(heads // 2):
                even = acc_s[i, (2 * pair) * BLOCK:(2 * pair + 1) * BLOCK, :]
                odd = acc_s[i, (2 * pair + 1) * BLOCK:(2 * pair + 2) * BLOCK, :]
                top = jnp.where(low, pltpu.roll(even, HEAD_DIM, 1), odd)
                bottom = jnp.where(low, even, pltpu.roll(odd, HEAD_DIM, 1))
                att[d, b * BLOCK:(b + 1) * BLOCK, pair * 128:(pair + 1) * 128] = (top / bottom).astype(jnp.bfloat16)
        if turn < n_tp - 1:
            att_copy(t, d).start()
        if turn + 1 < CHUNKS:
            pass_late(turn + 1)

    pass_last(0)
    pass_last(1)
    loads[5].wait()
    own_copy(near).wait_recv()
    att_copy(near, near).wait_recv()
    span = 512
    spans = [slice(col, col + span) for col in range(0, o_ref.shape[1], span)]
    for cols in spans:
        total = jnp.dot(att[t], wfull[t, :, cols], preferred_element_type=jnp.float32)
        total_s[:, cols] = total + jnp.dot(att_in[near], wfull[near, :, cols], preferred_element_type=jnp.float32)
    for c in range(2, CHUNKS):
        pass_last(c)

    for c in range(CHUNKS):
        for kind in range(4):
            near_copy(kind, c, far_near).wait_recv()
    for u in (far, far_near):
        att_copy(u, u).wait_recv()
    for cols in spans:
        total = total_s[:, cols] + jnp.dot(att_in[far], wfull[far, :, cols], preferred_element_type=jnp.float32)
        total += jnp.dot(att_in[far_near], wfull[far_near, :, cols], preferred_element_type=jnp.float32)
        o_ref[:, cols] = total.astype(jnp.bfloat16)

    own_copy(t).wait_send()
    for c in range(CHUNKS):
        x_copy(0, c, t).wait_send()
        link_copy(1, c, mine).wait_send()
        link_copy(2, c, mine).wait_send()
        if c < CHUNKS // 2:
            link_copy(3, c, from_z if c % 2 == 0 else from_y).wait_send()
        else:
            x_copy(3, c, t).wait_send()
        for kind in range(4):
            near_copy(kind, c, far).wait_send()
    for s in range(n - 1):
        @pl.when(s < me)
        def _():
            sel_copy(me, s).wait_send()
    for r in range(1, n):
        @pl.when(r > me)
        def _():
            kv_copy(me, r).wait_send()
    for d in (far, far_near, near):
        att_copy(t, d).wait_send()


def solution(mesh):
    n, n_tp, n_grp = mesh.shape["kv"], mesh.shape["tp"], mesh.shape["grp"]
    assert n_tp == 4 and n_grp == 2 and n % 2 == 0

    def shards(tokens, w_query, w_key, w_value, w_out, selection):
        rows, depth = tokens.shape
        q_width, width = w_query.shape[1], w_out.shape[1]
        blocks, topk = selection.shape[1:]
        heads = q_width // HEAD_DIM
        inside, outside = tables(n * blocks)
        bf, f32 = jnp.bfloat16, jnp.float32
        hbm = pl.BlockSpec(memory_space=pl.ANY)
        vmem = pl.BlockSpec(memory_space=pltpu.VMEM)
        dma = pltpu.SemaphoreType.DMA
        out_rows = rows // n_tp
        return pl.pallas_call(
            functools.partial(kernel, n, n_tp, n_grp),
            out_shape=pltpu.VMEM((out_rows, width), bf),
            in_specs=[hbm] * 8,
            out_specs=vmem,
            scratch_shapes=[
                pltpu.VMEM(inside.shape, f32),
                pltpu.VMEM(outside.shape, f32),
                pltpu.VMEM((rows, depth), bf),
                pltpu.VMEM((depth, q_width), bf),
                pltpu.VMEM((2 * HEAD_DIM, depth), bf),
                pltpu.VMEM((n_tp, q_width, width), bf),
                pltpu.VMEM((n, blocks, topk), jnp.int32),
                pltpu.VMEM((rows, q_width), f32),
                pltpu.VMEM((rows, 128), bf),
                pltpu.VMEM((n, 128, 128), bf),
                pltpu.VMEM((n - 1, 128, 128), bf),
                pltpu.VMEM((blocks, rows), f32),
                pltpu.VMEM((n - 1, blocks, 128), f32),
                pltpu.VMEM((blocks, heads * BLOCK, 128), f32),
                pltpu.VMEM((blocks, heads * BLOCK, 128), f32),
                pltpu.VMEM((blocks, heads * BLOCK, 128), bf),
                pltpu.VMEM((n_tp, out_rows, q_width), bf),
                pltpu.VMEM((n_tp, out_rows, q_width), bf),
                pltpu.VMEM((out_rows, width), f32),
                dma((7 + TOK_PARTS,)),
                dma((n,)), dma((n,)), dma((n,)), dma((n,)),
                dma((4, CHUNKS)), dma((4, CHUNKS)), dma, dma, dma((4, CHUNKS)), dma((4, CHUNKS)),
                dma((n_tp,)), dma((n_tp,)),
            ],
            compiler_params=pltpu.CompilerParams(
                collective_id=0, has_side_effects=True, vmem_limit_bytes=60 * 1024 * 1024
            ),
        )(tokens, w_query, w_key.T, w_value.T, w_out, selection, inside, outside)

    placed = (
        P(("grp", "kv"), None),
        P(None, "tp"),
        P(None, "tp"),
        P(None, "tp"),
        P("tp", None),
        P("tp", ("grp", "kv"), None),
    )
    return jax.shard_map(
        shards, mesh=mesh, in_specs=placed, out_specs=P(("grp", "kv", "tp"), None), check_vma=False
    )
```

profile of v0, /device:TPU:1, one launch (start us, length us, event | category | flops | bytes accessed | tf_op | source)
XLA Modules:
  0.0 22.7 jit_solution(14105052828687558627)
XLA Ops:
  0.0 21.9 %shard_map.82 = bf16[128,2048]{1,0:T(8,128)(2,1)S(1)} custom-call(bf16[512,2048]{1,0:T(8,128)(2,1)} %tok_h.1, bf16[2048,256]{1,0:T(8,128)(2,1)} %wq_h.1, bf16[64,2048]{1,0:T(8,128)(2,1)} %bitcast.2, bf16[64,2048]{1,0:T(8,128)(2,1)} %bitcast.3, bf16[256,2048]{1,0:T(8,128)(2,1)} %wo_h.1, s32[1,8,32]{2,1,0:T(8,128)} %sel_h.1, ...), custom_call_target="tpu_custom_call" | custom-call | tf_op jit(solution)/shard_map/pallas_call | solution.py:376
  21.9 0.8 %copy.10 = bf16[128,2048]{1,0:T(8,128)(2,1)} copy(bf16[128,2048]{1,0:T(8,128)(2,1)S(1)} %shard_map.82) | data formatting | bytes 1048576
where the time goes:
time: 22.8 us; the launch traced here: 22.7 us
  Pallas kernels  21.9 us (96%)
  local copies, waits for them, and re-layouts  0.8 us (4%)
    pallas_call x1, Pallas kernels, shards(): pl.pallas_call(functools.partial(kernel, n, n_tp, n_grp), out_shape=pltpu...  21.9 us
    unnamed x1, local copies, waits for them, and re-layouts  0.8 us

commit v1 on v0

--- a/solution.py
+++ b/solution.py
@@ -12,7 +12,8 @@
 BLOCK = 64
 ROPE_BASE = 500000.0
 NEG = -1e30
-CHUNKS = 4
+CUTS = (0, 1, 2, 4, 6, 8)
+LATE = ((0, 1), (2,), (3,), (4,))
 TOK_PARTS = 4
 MESH = pl.DeviceIdType.MESH
 NT = (((1,), (1,)), ((), ()))
@@ -25,18 +26,17 @@
     sign = np.where(lane % HEAD_DIM < half, -1.0, 1.0)
     inner = np.arange(BLOCK)[:, None] * freqs
     outer = (np.arange(n_blocks) * BLOCK)[:, None] * freqs
-    inside = np.stack([np.cos(inner), np.sin(inner), sign * np.cos(inner), sign * np.sin(inner)])
-    outside = np.stack([np.cos(outer), np.sin(outer)])
-    return inside.astype(np.float32), outside.astype(np.float32)
+    inside = [np.cos(inner), np.sin(inner), sign * np.cos(inner), sign * np.sin(inner)]
+    return np.concatenate(inside + [np.cos(outer), np.sin(outer)]).astype(np.float32)
 
 
 def kernel(
     n, n_tp, n_grp,
-    tok_h, wq_h, wk_h, wv_h, wo_h, sel_h, in_h, out_tab_h,
+    tok_h, wq_h, wk_h, wv_h, wo_h, sel_h, tab_h,
     o_ref,
-    in_ref, out_tab_ref, tok, wq, w_kv, wfull, sel_all, qf, kv_own, send_kv, recv_kv,
+    tab, tok, wq, w_kv, wfull, sel_all, qf, kv_own, send_kv, recv_kv,
     bias_l, bias_r, acc_s, max_s, qs_s, att, att_in, total_s,
-    in_sem, sel_ss, sel_rs, kv_ss, kv_rs, w_ss, w_rs, d_ss, d_rs, near_ss, near_rs, a_ss, a_rs,
+    in_sem, sel_ss, sel_rs, kv_ss, kv_rs, w_ss, x_rs, l_rs, own_rs, near_rs, a_ss, a_rs,
 ):
     grp = lax.axis_index("grp")
     me = lax.axis_index("kv")
@@ -53,24 +53,32 @@
     side = lax.rem(me, 2)
     beside = me + 1 - 2 * side
     mine, from_y, from_z, last_part = grp * 2 + side, other * 2 + side, grp * 2 + 1 - side, other * 2 + 1 - side
-    parts = (mine, from_y, from_z, last_part)
     quarter = width // (2 * n_grp)
-    piece = quarter // CHUNKS
+    unit = quarter // CUTS[-1]
     tok_rows = rows // TOK_PARTS
+    late_of = [k for k, group in enumerate(LATE) for c in group]
 
     def local(src, dst, k):
         return pltpu.make_async_copy(src, dst, in_sem.at[k])
 
-    loads = [
-        local(wk_h, w_kv.at[:HEAD_DIM], 0), local(wv_h, w_kv.at[HEAD_DIM:], 1), local(in_h, in_ref, 2),
-        local(sel_h.at[0], sel_all.at[me], 3), local(wq_h, wq, 4), local(wo_h, wfull.at[t], 5),
-        local(out_tab_h, out_tab_ref, 6),
+    def part_rows(part_of, lo=0, hi=CUTS[-1]):
+        return pl.ds(part_of * quarter + lo * unit, (hi - lo) * unit)
+
+    def w_load(part_of, k):
+        return local(wo_h.at[part_rows(part_of)], wfull.at[t, part_rows(part_of)], k)
+
+    sel_load = local(sel_h.at[0], sel_all.at[me], 0)
+    w_first, w_second = w_load(mine, 1), w_load(last_part, 2)
+    kv_loads = [
+        local(wk_h, w_kv.at[:HEAD_DIM], 3), local(wv_h, w_kv.at[HEAD_DIM:], 3), local(tab_h, tab, 5 + TOK_PARTS),
     ]
     tok_loads = []
     for k in range(TOK_PARTS):
         part = pl.ds(k * tok_rows, tok_rows)
-        tok_loads.append(local(tok_h.at[part], tok.at[part], 7 + k))
-    for load in loads[:2] + tok_loads + [loads[2], loads[6], loads[3], loads[4]]:
+        tok_loads.append(local(tok_h.at[part], tok.at[part], 5 + k))
+    q_load = local(wq_h, wq, 4)
+    w_rest = [w_load(from_y, 1), w_load(from_z, 1)]
+    for load in [sel_load, w_first, *kv_loads, tok_loads[0], w_second, *tok_loads[1:], q_load]:
         load.start()
 
     barrier = pltpu.get_barrier_semaphore()
@@ -78,9 +86,14 @@
         pl.semaphore_signal(barrier, inc=1, device_id={"tp": lax.rem(t + k, n_tp)}, device_id_type=MESH)
     for k in range(1, n_grp):
         pl.semaphore_signal(barrier, inc=1, device_id={"grp": lax.rem(grp + k, n_grp)}, device_id_type=MESH)
-    for k in range(1, n):
-        pl.semaphore_signal(barrier, inc=1, device_id={"kv": lax.rem(me + k, n)}, device_id_type=MESH)
-    pl.semaphore_wait(barrier, n_tp + n_grp + n - 3)
+    for r in range(1, n):
+        @pl.when(r > me)
+        def _():
+            pl.semaphore_signal(barrier, inc=1, device_id={"kv": r}, device_id_type=MESH)
+
+    @pl.when(side == 1)
+    def _():
+        pl.semaphore_signal(barrier, inc=1, device_id={"kv": beside}, device_id_type=MESH)
 
     def remote(src, dst, ss, rs, axis, index):
         return pltpu.make_async_remote_copy(
@@ -88,40 +101,80 @@
             device_id={axis: index}, device_id_type=MESH,
         )
 
-    def piece_of(part_of, c):
-        return pl.ds(part_of * quarter + c * piece, piece)
-
-    def x_copy(kind, c, owner):
-        at = piece_of(parts[kind], c)
-        return remote(wo_h.at[at], wfull.at[owner, at], w_ss.at[kind, c], w_rs.at[kind, c], "tp", far)
-
-    def link_copy(kind, c, part_of):
-        piece_at = wfull.at[far, piece_of(part_of, c)]
-        along_y = kind == 1 or (kind == 3 and c % 2 == 0)
-        axis, to = ("grp", other) if along_y else ("kv", beside)
-        return remote(piece_at, piece_at, w_ss.at[kind, c], w_rs.at[kind, c], axis, to)
-
-    def near_copy(kind, c, owner):
-        piece_at = wfull.at[owner, piece_of(parts[kind], c)]
-        return remote(piece_at, piece_at, near_ss.at[kind, c], near_rs.at[kind, c], "tp", near)
+    def x_copy(c, owner):
+        at = part_rows(mine, CUTS[c], CUTS[c + 1])
+        return remote(wfull.at[owner, at], wfull.at[owner, at], w_ss, x_rs.at[c], "tp", far)
+
+    def x_last(owner):
+        at = part_rows(last_part, CUTS[-1] // 2)
+        return remote(wfull.at[owner, at], wfull.at[owner, at], w_ss, x_rs.at[len(CUTS) - 1], "tp", far)
+
+    def link_copy(axis, to, part_of, lo, hi, k):
+        at = wfull.at[far, part_rows(part_of, lo, hi)]
+        return remote(at, at, w_ss, l_rs.at[k], axis, to)
+
+    def y_copy(c, part_of, k):
+        return link_copy("grp", other, part_of, CUTS[c], CUTS[c + 1], k)
+
+    def z_copy(c, part_of, k):
+        return link_copy("kv", beside, part_of, CUTS[c], CUTS[c + 1], k)
+
+    def y_last(part_of):
+        return link_copy("grp", other, part_of, 0, CUTS[-1] // 4, len(LATE))
+
+    def z_last(part_of):
+        return link_copy("kv", beside, part_of, CUTS[-1] // 4, CUTS[-1] // 2, len(LATE))
+
+    def near_copy(part_of, lo, hi):
+        at = wfull.at[far, part_rows(part_of, lo, hi)]
+        return remote(at, at, w_ss, near_rs, "tp", near)
 
     def own_copy(owner):
-        return remote(wo_h, wfull.at[owner], d_ss, d_rs, "tp", near)
+        return remote(wfull.at[owner], wfull.at[owner], w_ss, own_rs, "tp", near)
 
     def sel_copy(source, to):
-        return remote(sel_h.at[0], sel_all.at[source], sel_ss.at[to], sel_rs.at[source], "kv", to)
+        return remote(sel_all.at[source], sel_all.at[source], sel_ss, sel_rs.at[source], "kv", to)
 
     def kv_copy(source, to):
-        return remote(send_kv.at[to], recv_kv.at[source], kv_ss.at[to], kv_rs.at[source], "kv", to)
-
+        return remote(send_kv.at[to], recv_kv.at[source], kv_ss, kv_rs.at[source], "kv", to)
+
+    def pass_on(c):
+        x_copy(c, far).wait_recv()
+        y_copy(c, mine, late_of[c]).start()
+        z_copy(c, mine, late_of[c]).start()
+        near_copy(mine, CUTS[c], CUTS[c + 1]).start()
+
+    def pass_late(k):
+        lo, hi = CUTS[LATE[k][0]], CUTS[LATE[k][-1] + 1]
+        link_copy("grp", other, 0, 0, 2 * (hi - lo), k).wait_recv()
+        if k == 0:
+            y_last(from_z).start()
+        if k == 1:
+            z_last(from_y).start()
+        near_copy(from_y, lo, hi).start()
+        near_copy(from_z, lo, hi).start()
+
+    def pass_x_last():
+        x_last(far).wait_recv()
+        near_copy(last_part, CUTS[-1] // 2, CUTS[-1]).start()
+
+    def pass_last():
+        link_copy("grp", other, 0, 0, CUTS[-1] // 2, len(LATE)).wait_recv()
+        near_copy(last_part, 0, CUTS[-1] // 2).start()
+
+    sel_load.wait()
+    w_first.wait()
+    pl.semaphore_wait(barrier, n_tp + n_grp - 2 + me + 1 - side)
+    for c in range(len(CUTS) - 1):
+        x_copy(c, t).start()
     for s in range(n - 1):
         @pl.when(s < me)
         def _():
             sel_copy(me, s).start()
-    for c in range(CHUNKS):
-        x_copy(0, c, t).start()
-    for c in range(CHUNKS // 2, CHUNKS):
-        x_copy(3, c, t).start()
+    w_second.wait()
+    x_last(t).start()
+    for load in w_rest:
+        load.start()
 
     for s in range(n - 1):
         @pl.when(s >= me)
@@ -133,19 +186,18 @@
     first = lax.rem(lane, HEAD_DIM) < HEAD_DIM // 2
 
     def angle(i):
-        at = me * blocks + i
-        cos_b = out_tab_ref[0, pl.ds(at, 1), :]
-        sin_b = out_tab_ref[1, pl.ds(at, 1), :]
-        return in_ref[0] * cos_b - in_ref[1] * sin_b, in_ref[3] * cos_b + in_ref[2] * sin_b
+        at = 4 * BLOCK + me * blocks + i
+        cos_b = tab[pl.ds(at, 1), :]
+        sin_b = tab[pl.ds(at + n * blocks, 1), :]
+        cos_i, sin_i, cos_s, sin_s = (tab[k * BLOCK:(k + 1) * BLOCK, :] for k in range(4))
+        return cos_i * cos_b - sin_i * sin_b, sin_s * cos_b + cos_s * sin_b
 
     def rotated(x, cos, sin):
         swapped = jnp.where(first, pltpu.roll(x, 96, 1), pltpu.roll(x, 32, 1))
         return x * cos + swapped * sin
 
-    loads[0].wait()
-    loads[1].wait()
-    loads[2].wait()
-    loads[6].wait()
+    local(w_kv, w_kv, 3).wait()
+    kv_loads[2].wait()
     per_part = tok_rows // BLOCK
     for i in range(blocks):
         if i % per_part == 0:
@@ -169,7 +221,6 @@
         hi = jnp.max(jnp.max(hi, axis=1, keepdims=True), axis=0, keepdims=True)
         return lo, hi
 
-    loads[3].wait()
     r_iota = lax.broadcasted_iota(jnp.int32, (2 * BLOCK, rows), 0)
     c_iota = lax.broadcasted_iota(jnp.int32, (2 * BLOCK, rows), 1)
     r_in = lax.rem(r_iota, BLOCK).astype(jnp.float32)
@@ -185,12 +236,15 @@
             send_kv[r] = chosen.astype(jnp.bfloat16)
             kv_copy(me, r).start()
 
-    loads[5].start()
+    both = pl.ds(0, 2 * quarter)
+    local(wo_h.at[both], wfull.at[t, both], 1).wait()
     own_copy(t).start()
-
-    loads[4].wait()
+    pass_on(0)
+
+    q_load.wait()
     qf[...] = jnp.dot(tok[...], wq[...], preferred_element_type=jnp.float32)
 
+    pass_on(1)
     sel_f = sel_all[me].astype(jnp.float32)
     base = (me * blocks).astype(jnp.float32)
     local_id = (lax.broadcasted_iota(jnp.int32, (blocks, rows), 1) // BLOCK).astype(jnp.float32) + base
@@ -216,28 +270,6 @@
     q_col = lax.broadcasted_iota(jnp.int32, (group_rows, 128), 1)
     zero = jnp.zeros((BLOCK, 128), jnp.float32)
 
-    def pass_on(c):
-        x_copy(0, c, far).wait_recv()
-        link_copy(1, c, mine).start()
-        link_copy(2, c, mine).start()
-        near_copy(0, c, far).start()
-
-    def pass_late(c):
-        link_copy(1, c, from_y).wait_recv()
-        link_copy(2, c, from_z).wait_recv()
-        if c < CHUNKS // 2:
-            link_copy(3, c, from_z if c % 2 == 0 else from_y).start()
-        near_copy(1, c, far).start()
-        near_copy(2, c, far).start()
-
-    def pass_last(c):
-        if c < CHUNKS // 2:
-            link_copy(3, c, last_part).wait_recv()
-        else:
-            x_copy(3, c, far).wait_recv()
-        near_copy(3, c, far).start()
-
-    pass_on(0)
     for i in range(blocks):
         cos, sin = angle(i)
         cos, sin = cos * HEAD_DIM ** -0.5, sin * HEAD_DIM ** -0.5
@@ -258,8 +290,10 @@
         p = jnp.exp(scores - top).astype(jnp.bfloat16)
         acc_s[i] = jnp.dot(p, with_ones(kv), preferred_element_type=jnp.float32)
         max_s[i] = jnp.broadcast_to(top, (group_rows, 128))
-        if i % 2 == 1 and i // 2 + 1 < CHUNKS:
-            pass_on(i // 2 + 1)
+        if i == blocks // 4:
+            pass_on(2)
+        if i == blocks // 2 + 1:
+            pass_on(3)
     pass_late(0)
 
     for s in range(n - 1):
@@ -286,8 +320,8 @@
 
     per = blocks // n_tp
 
-    def att_copy(owner, to):
-        return remote(att.at[to], att_in.at[owner], a_ss.at[to], a_rs.at[owner], "tp", to)
+    def att_copy(owner, to, k):
+        return remote(att.at[to], att_in.at[owner], a_ss, a_rs.at[k], "tp", to)
 
     far_near = lax.rem(near + n_tp // 2, n_tp)
     for turn, d in enumerate((far, far_near, near, t)):
@@ -308,54 +342,40 @@
                 bottom = jnp.where(low, even, pltpu.roll(odd, HEAD_DIM, 1))
                 att[d, b * BLOCK:(b + 1) * BLOCK, pair * 128:(pair + 1) * 128] = (top / bottom).astype(jnp.bfloat16)
         if turn < n_tp - 1:
-            att_copy(t, d).start()
-        if turn + 1 < CHUNKS:
+            att_copy(t, d, turn // 2).start()
+        if turn == 0:
+            pass_on(4)
+        if turn < len(LATE) - 1:
             pass_late(turn + 1)
-
-    pass_last(0)
-    pass_last(1)
-    loads[5].wait()
+        if turn == 2:
+            pass_x_last()
+
+    pass_last()
     own_copy(near).wait_recv()
-    att_copy(near, near).wait_recv()
+    att_copy(near, near, 1).wait_recv()
     span = 512
     spans = [slice(col, col + span) for col in range(0, o_ref.shape[1], span)]
     for cols in spans:
         total = jnp.dot(att[t], wfull[t, :, cols], preferred_element_type=jnp.float32)
         total_s[:, cols] = total + jnp.dot(att_in[near], wfull[near, :, cols], preferred_element_type=jnp.float32)
-    for c in range(2, CHUNKS):
-        pass_last(c)
-
-    for c in range(CHUNKS):
-        for kind in range(4):
-            near_copy(kind, c, far_near).wait_recv()
-    for u in (far, far_near):
-        att_copy(u, u).wait_recv()
+
+    remote(wfull.at[far_near], wfull.at[far_near], w_ss, near_rs, "tp", near).wait_recv()
+    remote(att_in.at[:2], att_in.at[:2], a_ss, a_rs.at[0], "tp", near).wait_recv()
     for cols in spans:
         total = total_s[:, cols] + jnp.dot(att_in[far], wfull[far, :, cols], preferred_element_type=jnp.float32)
         total += jnp.dot(att_in[far_near], wfull[far_near, :, cols], preferred_element_type=jnp.float32)
         o_ref[:, cols] = total.astype(jnp.bfloat16)
 
-    own_copy(t).wait_send()
-    for c in range(CHUNKS):
-        x_copy(0, c, t).wait_send()
-        link_copy(1, c, mine).wait_send()
-        link_copy(2, c, mine).wait_send()
-        if c < CHUNKS // 2:
-            link_copy(3, c, from_z if c % 2 == 0 else from_y).wait_send()
-        else:
-            x_copy(3, c, t).wait_send()
-        for kind in range(4):
-            near_copy(kind, c, far).wait_send()
-    for s in range(n - 1):
-        @pl.when(s < me)
-        def _():
-            sel_copy(me, s).wait_send()
-    for r in range(1, n):
-        @pl.when(r > me)
-        def _():
-            kv_copy(me, r).wait_send()
-    for d in (far, far_near, near):
-        att_copy(t, d).wait_send()
+    remote(wfull.at[:3], wfull.at[:3], w_ss, near_rs, "tp", near).wait_send()
+    remote(att.at[:3], att.at[:3], a_ss, near_rs, "tp", near).wait_send()
+    for k in range(1, n):
+        @pl.when(me == k)
+        def _():
+            remote(sel_all.at[:k], sel_all.at[:k], sel_ss, sel_rs.at[0], "kv", beside).wait_send()
+
+        @pl.when(me == n - 1 - k)
+        def _():
+            remote(send_kv.at[:k], send_kv.at[:k], kv_ss, kv_rs.at[0], "kv", beside).wait_send()
 
 
 def solution(mesh):
@@ -367,7 +387,7 @@
         q_width, width = w_query.shape[1], w_out.shape[1]
         blocks, topk = selection.shape[1:]
         heads = q_width // HEAD_DIM
-        inside, outside = tables(n * blocks)
+        table = tables(n * blocks)
         bf, f32 = jnp.bfloat16, jnp.float32
         hbm = pl.BlockSpec(memory_space=pl.ANY)
         vmem = pl.BlockSpec(memory_space=pltpu.VMEM)
@@ -376,11 +396,10 @@
         return pl.pallas_call(
             functools.partial(kernel, n, n_tp, n_grp),
             out_shape=pltpu.VMEM((out_rows, width), bf),
-            in_specs=[hbm] * 8,
+            in_specs=[hbm] * 7,
             out_specs=vmem,
             scratch_shapes=[
-                pltpu.VMEM(inside.shape, f32),
-                pltpu.VMEM(outside.shape, f32),
+                pltpu.VMEM(table.shape, f32),
                 pltpu.VMEM((rows, depth), bf),
                 pltpu.VMEM((depth, q_width), bf),
                 pltpu.VMEM((2 * HEAD_DIM, depth), bf),
@@ -398,15 +417,14 @@
                 pltpu.VMEM((n_tp, out_rows, q_width), bf),
                 pltpu.VMEM((n_tp, out_rows, q_width), bf),
                 pltpu.VMEM((out_rows, width), f32),
-                dma((7 + TOK_PARTS,)),
-                dma((n,)), dma((n,)), dma((n,)), dma((n,)),
-                dma((4, CHUNKS)), dma((4, CHUNKS)), dma, dma, dma((4, CHUNKS)), dma((4, CHUNKS)),
-                dma((n_tp,)), dma((n_tp,)),
+                dma((6 + TOK_PARTS,)),
+                dma, dma((n,)), dma, dma((n - 1,)),
+                dma, dma((len(CUTS),)), dma((len(LATE) + 1,)), dma, dma, dma, dma((2,)),
             ],
             compiler_params=pltpu.CompilerParams(
                 collective_id=0, has_side_effects=True, vmem_limit_bytes=60 * 1024 * 1024
             ),
-        )(tokens, w_query, w_key.T, w_value.T, w_out, selection, inside, outside)
+        )(tokens, w_query, w_key.T, w_value.T, w_out, selection, table)
 
     placed = (
         P(("grp", "kv"), None),

time: 22.8 us -> 22.2 us (0.974)
  Pallas kernels: 21.9 us -> 21.2 us
    pallas_call x1, Pallas kernels: 21.9 us -> 21.2 us  [shards(): pl.pallas_call(functools.partial(kernel, n, n_tp, n_grp), out_shape=pltpu...]
where the time goes in v1:
time: 22.2 us; the launch traced here: 22 us
  Pallas kernels  21.2 us (95%)
  local copies, waits for them, and re-layouts  0.8 us (4%)
    pallas_call x1, Pallas kernels, shards(): pl.pallas_call(functools.partial(kernel, n, n_tp, n_grp), out_shape=pltpu...  21.2 us
    unnamed x1, local copies, waits for them, and re-layouts  0.8 us

profile of v1, /device:TPU:1, one launch (start us, length us, event | category | flops | bytes accessed | tf_op | source)
XLA Modules:
  0.0 22.0 jit_solution(11184230029489822822)
XLA Ops:
  0.0 21.2 %shard_map.73 = bf16[128,2048]{1,0:T(8,128)(2,1)S(1)} custom-call(bf16[512,2048]{1,0:T(8,128)(2,1)} %tok_h.1, bf16[2048,256]{1,0:T(8,128)(2,1)} %wq_h.1, bf16[64,2048]{1,0:T(8,128)(2,1)} %bitcast.2, bf16[64,2048]{1,0:T(8,128)(2,1)} %bitcast.3, bf16[256,2048]{1,0:T(8,128)(2,1)} %wo_h.1, s32[1,8,32]{2,1,0:T(8,128)} %sel_h.1, f32[320,128]{1,0:T(8,128)} %constant.2.clone.tab_h), custom_call_target="tpu_custom_call" | custom-call | tf_op jit(solution)/shard_map/pallas_call | solution.py:396
  21.2 0.8 %copy.9 = bf16[128,2048]{1,0:T(8,128)(2,1)} copy(bf16[128,2048]{1,0:T(8,128)(2,1)S(1)} %shard_map.73) | data formatting | bytes 1048576

commit v2 on v1

--- a/solution.py
+++ b/solution.py
@@ -14,7 +14,9 @@
 NEG = -1e30
 CUTS = (0, 1, 2, 4, 6, 8)
 LATE = ((0, 1), (2,), (3,), (4,))
-TOK_PARTS = 4
+TOK_PARTS = 2
+ON, ANSWER = 0, 1
+STEPS = {2: ((ANSWER, 1), (ON, 0), (ON, 1)), 3: ((ANSWER, 2),), 4: ((ANSWER, 3), (ON, 2)), 6: ((ON, 3),)}
 MESH = pl.DeviceIdType.MESH
 NT = (((1,), (1,)), ((), ()))
 
@@ -34,7 +36,7 @@
     n, n_tp, n_grp,
     tok_h, wq_h, wk_h, wv_h, wo_h, sel_h, tab_h,
     o_ref,
-    tab, tok, wq, w_kv, wfull, sel_all, qf, kv_own, send_kv, recv_kv,
+    tab, tok, w_qkv, w_kv, wfull, sel_all, qf, kv_own, send_kv, recv_kv,
     bias_l, bias_r, acc_s, max_s, qs_s, att, att_in, total_s,
     in_sem, sel_ss, sel_rs, kv_ss, kv_rs, w_ss, x_rs, l_rs, own_rs, near_rs, a_ss, a_rs,
 ):
@@ -43,7 +45,8 @@
     t = lax.axis_index("tp")
     rows = tok.shape[0]
     blocks = rows // BLOCK
-    heads = wq.shape[1] // HEAD_DIM
+    q_width = wq_h.shape[1]
+    heads = q_width // HEAD_DIM
     topk = sel_all.shape[2]
     group_rows = heads * BLOCK
     far = lax.rem(t + n_tp // 2, n_tp)
@@ -76,9 +79,9 @@
     for k in range(TOK_PARTS):
         part = pl.ds(k * tok_rows, tok_rows)
         tok_loads.append(local(tok_h.at[part], tok.at[part], 5 + k))
-    q_load = local(wq_h, wq, 4)
+    q_load = local(wq_h, w_qkv.at[:, :q_width], 4)
     w_rest = [w_load(from_y, 1), w_load(from_z, 1)]
-    for load in [sel_load, w_first, *kv_loads, tok_loads[0], w_second, *tok_loads[1:], q_load]:
+    for load in [sel_load, w_first, *kv_loads, q_load, tok_loads[0], w_second, *tok_loads[1:]]:
         load.start()
 
     barrier = pltpu.get_barrier_semaphore()
@@ -171,10 +174,6 @@
         @pl.when(s < me)
         def _():
             sel_copy(me, s).start()
-    w_second.wait()
-    x_last(t).start()
-    for load in w_rest:
-        load.start()
 
     for s in range(n - 1):
         @pl.when(s >= me)
@@ -197,19 +196,25 @@
         return x * cos + swapped * sin
 
     local(w_kv, w_kv, 3).wait()
+    w_qkv[:, q_width:] = w_kv[...].T
+    w_second.wait()
+    x_last(t).start()
+    for load in w_rest:
+        load.start()
     kv_loads[2].wait()
+    q_load.wait()
     per_part = tok_rows // BLOCK
-    for i in range(blocks):
-        if i % per_part == 0:
-            tok_loads[i // per_part].wait()
-            at = i * BLOCK
-            qf[at:at + tok_rows, :128] = lax.dot_general(
-                tok[at:at + tok_rows, :], w_kv[...], NT, preferred_element_type=jnp.float32
-            )
-        cos, sin = angle(i)
-        x = qf[i * BLOCK:(i + 1) * BLOCK, :128]
-        turned = rotated(x, jnp.where(low, cos, 1.0), jnp.where(low, sin, 0.0))
-        kv_own[i * BLOCK:(i + 1) * BLOCK, :] = turned.astype(jnp.bfloat16)
+    for k in range(TOK_PARTS):
+        tok_loads[k].wait()
+        part = slice(k * tok_rows, (k + 1) * tok_rows)
+        found = jnp.dot(tok[part, :], w_qkv[...], preferred_element_type=jnp.float32)
+        qf[part, :] = found[:, :q_width]
+        for b in range(per_part):
+            i = k * per_part + b
+            cos, sin = angle(i)
+            x = found[b * BLOCK:(b + 1) * BLOCK, q_width:]
+            turned = rotated(x, jnp.where(low, cos, 1.0), jnp.where(low, sin, 0.0))
+            kv_own[i * BLOCK:(i + 1) * BLOCK, :] = turned.astype(jnp.bfloat16)
 
     def ends(sel, source):
         e = sel - source * blocks
@@ -225,9 +230,14 @@
     c_iota = lax.broadcasted_iota(jnp.int32, (2 * BLOCK, rows), 1)
     r_in = lax.rem(r_iota, BLOCK).astype(jnp.float32)
     c_f = c_iota.astype(jnp.float32)
-    for r in range(n - 1, 0, -1):
-        @pl.when(r > me)
-        def _():
+
+    def answer(dist):
+        if dist >= n:
+            return
+
+        @pl.when(me + dist < n)
+        def _():
+            r = me + dist
             sel_copy(r, r).wait_recv()
             lo, hi = ends(sel_all[r], me)
             want = jnp.where(r_iota < BLOCK, lo, hi) * BLOCK + r_in
@@ -239,12 +249,7 @@
     both = pl.ds(0, 2 * quarter)
     local(wo_h.at[both], wfull.at[t, both], 1).wait()
     own_copy(t).start()
-    pass_on(0)
-
-    q_load.wait()
-    qf[...] = jnp.dot(tok[...], wq[...], preferred_element_type=jnp.float32)
-
-    pass_on(1)
+
     sel_f = sel_all[me].astype(jnp.float32)
     base = (me * blocks).astype(jnp.float32)
     local_id = (lax.broadcasted_iota(jnp.int32, (blocks, rows), 1) // BLOCK).astype(jnp.float32) + base
@@ -290,10 +295,10 @@
         p = jnp.exp(scores - top).astype(jnp.bfloat16)
         acc_s[i] = jnp.dot(p, with_ones(kv), preferred_element_type=jnp.float32)
         max_s[i] = jnp.broadcast_to(top, (group_rows, 128))
-        if i == blocks // 4:
-            pass_on(2)
-        if i == blocks // 2 + 1:
-            pass_on(3)
+        for step, k in STEPS.get(i, ()):
+            (pass_on, answer)[step](k)
+    for dist in range(4, n):
+        answer(dist)
     pass_late(0)
 
     for s in range(n - 1):
@@ -303,11 +308,11 @@
 
     step = max(k for k in (1, 2, 3, 4) if (n - 1) % k == 0)
 
-    def remote_part(at, i):
-        kv = recv_kv[pl.ds(at * step, step)].reshape(step * 128, 128)
+    def remote_part(at, i, count):
+        kv = recv_kv[pl.ds(at, count)].reshape(count * 128, 128)
         scores = lax.dot_general(qs_s[i], kv, NT, preferred_element_type=jnp.float32)
         scores = jnp.concatenate(
-            [scores[:, k * 128:(k + 1) * 128] + bias_r[at * step + k, pl.ds(i, 1), :] for k in range(step)], axis=1
+            [scores[:, k * 128:(k + 1) * 128] + bias_r[at + k, pl.ds(i, 1), :] for k in range(count)], axis=1
         )
         before = max_s[i]
         top = jnp.maximum(before[:, :1], jnp.max(scores, axis=1, keepdims=True))
@@ -318,6 +323,20 @@
         if n - 1 > step:
             max_s[i] = jnp.broadcast_to(top, (group_rows, 128))
 
+    def remote_parts(many):
+        if n - 1 > step:
+            @pl.when(me > 0)
+            def _():
+                for i in many:
+                    lax.fori_loop(0, (n - 1) // step, lambda at, _: (remote_part(at * step, i, step), 0)[1], 0)
+        else:
+            for count in range(1, n):
+                @pl.when(me == count)
+                def _():
+                    for i in many:
+                        remote_part(0, i, count)
+
+    pass_on(4)
     per = blocks // n_tp
 
     def att_copy(owner, to, k):
@@ -325,16 +344,9 @@
 
     far_near = lax.rem(near + n_tp // 2, n_tp)
     for turn, d in enumerate((far, far_near, near, t)):
+        remote_parts([d * per + b for b in range(per)])
         for b in range(per):
             i = d * per + b
-
-            @pl.when(me > 0)
-            def _():
-                if n - 1 > step:
-                    lax.fori_loop(0, (n - 1) // step, lambda at, _: (remote_part(at, i), 0)[1], 0)
-                else:
-                    remote_part(0, i)
-
             for pair in range(heads // 2):
                 even = acc_s[i, (2 * pair) * BLOCK:(2 * pair + 1) * BLOCK, :]
                 odd = acc_s[i, (2 * pair + 1) * BLOCK:(2 * pair + 2) * BLOCK, :]
@@ -343,8 +355,6 @@
                 att[d, b * BLOCK:(b + 1) * BLOCK, pair * 128:(pair + 1) * 128] = (top / bottom).astype(jnp.bfloat16)
         if turn < n_tp - 1:
             att_copy(t, d, turn // 2).start()
-        if turn == 0:
-            pass_on(4)
         if turn < len(LATE) - 1:
             pass_late(turn + 1)
         if turn == 2:
@@ -401,7 +411,7 @@
             scratch_shapes=[
                 pltpu.VMEM(table.shape, f32),
                 pltpu.VMEM((rows, depth), bf),
-                pltpu.VMEM((depth, q_width), bf),
+                pltpu.VMEM((depth, q_width + 2 * HEAD_DIM), bf),
                 pltpu.VMEM((2 * HEAD_DIM, depth), bf),
                 pltpu.VMEM((n_tp, q_width, width), bf),
                 pltpu.VMEM((n, blocks, topk), jnp.int32),

time: 22.2 us -> 19.7 us (0.89)
  Pallas kernels: 21.2 us -> 18.7 us
    pallas_call x1, Pallas kernels: 21.2 us -> 18.7 us  [shards(): pl.pallas_call(functools.partial(kernel, n, n_tp, n_grp), out_shape=pltpu...]
where the time goes in v2:
time: 19.7 us; the launch traced here: 19.5 us
  Pallas kernels  18.7 us (95%)
  local copies, waits for them, and re-layouts  0.8 us (4%)
    pallas_call x1, Pallas kernels, shards(): pl.pallas_call(functools.partial(kernel, n, n_tp, n_grp), out_shape=pltpu...  18.7 us
    unnamed x1, local copies, waits for them, and re-layouts  0.8 us

profile of v2, /device:TPU:1, one launch (start us, length us, event | category | flops | bytes accessed | tf_op | source)
XLA Modules:
  0.0 19.5 jit_solution(13784991570994123690)
XLA Ops:
  0.0 18.7 %shard_map.73 = bf16[128,2048]{1,0:T(8,128)(2,1)S(1)} custom-call(bf16[512,2048]{1,0:T(8,128)(2,1)} %tok_h.1, bf16[2048,256]{1,0:T(8,128)(2,1)} %wq_h.1, bf16[64,2048]{1,0:T(8,128)(2,1)} %bitcast.2, bf16[64,2048]{1,0:T(8,128)(2,1)} %bitcast.3, bf16[256,2048]{1,0:T(8,128)(2,1)} %wo_h.1, s32[1,8,32]{2,1,0:T(8,128)} %sel_h.1, f32[320,128]{1,0:T(8,128)} %constant.2.clone.tab_h), custom_call_target="tpu_custom_call" | custom-call | tf_op jit(solution)/shard_map/pallas_call | solution.py:406
  18.7 0.8 %copy.9 = bf16[128,2048]{1,0:T(8,128)(2,1)} copy(bf16[128,2048]{1,0:T(8,128)(2,1)S(1)} %shard_map.73) | data formatting | bytes 1048576
